TPU v7x, 128 devices: a whole 4x4x4 slice. The times are simulated.
128 devices in a mesh: ep: 64 (over z, y, x), tp: 2 (over core).
Axes of the slice: x: 4, y: 4, z: 4, core: 2. Of those that a mesh axis runs over, the one named last changes fastest.
Arguments:
- residual: bfloat16 [1024, 4096], P(('ep', 'tp')), may hold values from -6 to 6
- lengths: int32 [1024], P(('ep', 'tp')), may hold values from 128 to 1024
- latent_cache: bfloat16 [1024, 1024, 512], P(('ep', 'tp'))
- rope_cache: bfloat16 [1024, 1024, 64], P(('ep', 'tp')), may hold values from -6 to 6
- route_ids: int32 [1024, 2], P(('ep', 'tp')), may hold values from 0 to 7, all different within a row; in each aligned block of 8 rows (0 to 7, 8 to 15, ...) at most 3 rows name the same one
- route_scores: bfloat16 [1024, 2], P(('ep', 'tp')), may hold values from -6 to 6
- norm_first: float32 [4096], replicated, may hold values from 0.1 to 1.9
- norm_second: float32 [4096], replicated, may hold values from 0.1 to 1.9
- query_gain: float32 [1024], replicated, may hold values from 0.1 to 1.9
- latent_gain: float32 [512], replicated, may hold values from 0.1 to 1.9
- query_down: bfloat16 [4096, 1024], P(('ep', 'tp')), may hold values from -0.09375 to 0.09375
- latent_down: bfloat16 [4096, 512], P(('ep', 'tp')), may hold values from -0.09375 to 0.09375
- rope_down: bfloat16 [4096, 64], replicated, may hold values from -0.09375 to 0.09375
- query_latent: bfloat16 [1024, 16384], P(None, ('ep', 'tp')), may hold values from -0.1875 to 0.1875
- query_rope: bfloat16 [1024, 2048], P(None, ('ep', 'tp')), may hold values from -0.1875 to 0.1875
- value_up: bfloat16 [512, 32, 128], replicated, may hold values from -1 to 1
- output_weight: bfloat16 [4096, 4096], P(None, ('ep', 'tp')), may hold values from -0.09375 to 0.09375
- expert_gate: bfloat16 [4096, 57344], P(None, ('ep', 'tp')), may hold values from -0.09375 to 0.09375
- expert_up: bfloat16 [4096, 57344], P(None, ('ep', 'tp')), may hold values from -0.09375 to 0.09375
- expert_down: bfloat16 [57344, 4096], P(('ep', 'tp')), may hold values from -0.125 to 0.125
Outputs:
- layer_out: bfloat16 [1024, 4096], P(('ep', 'tp'))
- new_latent: bfloat16 [1024, 512], P(('ep', 'tp'))
- new_rope: bfloat16 [1024, 64], P(('ep', 'tp'))
Inputs may be any that keep to these rules, and one draw needn't show every extreme that they name: `route_ids`: each row names 2 different experts. Within the rows of one device (aligned blocks of 8 rows) no expert is named more than 3 times; in every draw some expert is named exactly 3 times in some blocks. `lengths`: A sequence's cached positions are 0 to its length - 1; the new token stands at position length.
All inputs are finite; a program needn't handle non-finite values.
Results may differ from a plain program's by a relative error of at most 0.014.
The roundings to bfloat16 on the way count: a program that leaves them out, or rounds other values in their place, can miss the bound.
Values may be sent and summed in bfloat16 or wider, within the bound.
A program may use at most 128 MiB of HBM per device.

v0:
```python
import jax
import jax.numpy as jnp
from jax import lax
from jax.sharding import Mesh
from jax.sharding import PartitionSpec as P

ROPE = 64
NOPE = 128
EXPERTS = 8
TOP = 2
CAP = 3
EP_TP = ("ep_0", "ep_1", "ep_2", "tp")
epsilon = 1e-06
rope_base = 10000.0


def cut_along(shard, dim, peers):
    before, after = (shard.shape[:dim], shard.shape[dim + 1 :])
    return jnp.moveaxis(shard.reshape(*before, peers, -1, *after), dim, 0)


def sent_and_summed(shard, axis, dim):
    parts = cut_along(shard, dim, lax.axis_size(axis))
    arrived = lax.all_to_all(parts, axis, split_axis=0, concat_axis=0, tiled=True)
    return arrived.sum(axis=0)


def sum_by_axis(shard, axes, dim):
    far, near = axes
    parts = cut_along(shard, dim, lax.axis_size(far))
    nearer = sent_and_summed(parts, near, dim + 1)
    arrived = lax.all_to_all(nearer, far, split_axis=0, concat_axis=0, tiled=True)
    return arrived.sum(axis=0)


def sent_to_all(shard, axis):
    peers = lax.axis_size(axis)
    return lax.all_to_all(
        jnp.broadcast_to(shard[None], (peers, *shard.shape)), axis, 0, 0, tiled=True
    )


def in_order(parts, dim):
    shape = list(parts.shape[1:])
    shape[dim] *= parts.shape[0]
    return jnp.moveaxis(parts, 0, dim).reshape(shape)


def gathered_by_axis(shard, axes, dim):
    far, near = axes
    parts = sent_to_all(sent_to_all(shard, far), near)
    return in_order(parts.swapaxes(0, 1).reshape(-1, *shard.shape), dim)


def normalize(values_in, gain_row):
    return (
        values_in
        * lax.rsqrt(jnp.mean(values_in * values_in, axis=-1, keepdims=True) + epsilon)
        * gain_row
    )


def rotate(values_in, turns):
    half_width = values_in.shape[-1] // 2
    front_half = values_in[..., :half_width]
    back_half = values_in[..., half_width:]
    cosine = jnp.cos(turns)
    sine_part = jnp.sin(turns)
    return jnp.concatenate(
        [front_half * cosine - back_half * sine_part, front_half * sine_part + back_half * cosine],
        axis=-1,
    )


def rotary_angles(positions, rotary_width):
    inverse = rope_base ** (-jnp.arange(0, rotary_width, 2, dtype=jnp.float32) / rotary_width)
    return positions.astype(jnp.float32)[:, None] * inverse[None, :]


def slot_tables(route_block):
    experts = jnp.arange(EXPERTS, dtype=jnp.int32)
    onehot = (route_block[..., None] == experts).astype(jnp.int32)
    earlier = jnp.cumsum(onehot, axis=-2) - onehot
    slot_rank = jnp.sum(earlier * onehot, axis=-1)
    places = jnp.arange(CAP, dtype=jnp.int32)
    return onehot[..., None] * (slot_rank[..., None, None] == places).astype(jnp.int32)


def owner_table(sequences):
    assign = sequences * TOP
    return (
        jnp.arange(assign, dtype=jnp.int32)[None, :] // TOP
        == jnp.arange(sequences, dtype=jnp.int32)[:, None]
    ).astype(jnp.float32)


def expert_rows(row_block, expert_gate, expert_up, expert_down):
    gate_part = jnp.dot(row_block, expert_gate, preferred_element_type=jnp.float32)
    up_part = jnp.dot(row_block, expert_up, preferred_element_type=jnp.float32)
    hidden = (jax.nn.silu(gate_part) * up_part).astype(jnp.bfloat16)
    return jnp.dot(hidden, expert_down, preferred_element_type=jnp.float32)


def attend_local(
    query_latents, query_rotary, latent_cache, rope_cache, new_latent, new_rope, lengths
):
    score_scale = (NOPE + ROPE) ** (-0.5)
    cache_scores = (
        jnp.einsum("shl,spl->shp", query_latents, latent_cache, preferred_element_type=jnp.float32)
        + jnp.einsum("shr,spr->shp", query_rotary, rope_cache, preferred_element_type=jnp.float32)
    ) * score_scale
    new_scores = (
        jnp.einsum("shl,sl->sh", query_latents, new_latent, preferred_element_type=jnp.float32)
        + jnp.einsum("shr,sr->sh", query_rotary, new_rope, preferred_element_type=jnp.float32)
    ) * score_scale
    visible = jnp.arange(latent_cache.shape[1], dtype=jnp.int32)[None, :] < lengths[:, None]
    cache_scores = jnp.where(visible[:, None, :], cache_scores, -jnp.inf)
    row_top = jnp.maximum(jnp.max(cache_scores, axis=-1), new_scores)
    cache_terms = jnp.exp(cache_scores - row_top[..., None])
    new_term = jnp.exp(new_scores - row_top)
    denominator = jnp.sum(cache_terms, axis=-1) + new_term
    cache_probs = (cache_terms / denominator[..., None]).astype(jnp.bfloat16)
    new_probs = (new_term / denominator).astype(jnp.bfloat16)
    mixture = jnp.einsum(
        "shp,spl->shl", cache_probs, latent_cache, preferred_element_type=jnp.float32
    )
    mixture = (
        mixture
        + new_probs.astype(jnp.float32)[..., None] * new_latent.astype(jnp.float32)[:, None, :]
    )
    return mixture.astype(jnp.bfloat16)


def local(
    residual,
    lengths,
    latent_cache,
    rope_cache,
    route_ids,
    route_scores,
    norm_first,
    norm_second,
    query_gain,
    latent_gain,
    query_down,
    latent_down,
    rope_down,
    query_latent,
    query_rope,
    value_up,
    output_weight,
    expert_gate,
    expert_up,
    expert_down,
):
    sequences = residual.shape[0]
    model_width = residual.shape[1]
    devices = lax.axis_size(EP_TP)
    stream = residual.astype(jnp.float32)
    normed = normalize(stream, norm_first).astype(jnp.bfloat16)
    slices = lax.all_to_all(normed, EP_TP, split_axis=1, concat_axis=0, tiled=True)
    query_width = query_down.shape[1]
    lowered = sum_by_axis(
        jnp.concatenate(
            [
                jnp.dot(slices, query_down, preferred_element_type=jnp.float32),
                jnp.dot(slices, latent_down, preferred_element_type=jnp.float32),
            ],
            axis=1,
        ),
        (("ep_0", "ep_1", "ep_2"), "tp"),
        0,
    )
    query_small = normalize(lowered[:, :query_width], query_gain).astype(jnp.bfloat16)
    new_latent = normalize(lowered[:, query_width:], latent_gain).astype(jnp.bfloat16)
    turns = rotary_angles(lengths, rope_down.shape[1])
    new_rope = rotate(jnp.dot(normed, rope_down, preferred_element_type=jnp.float32), turns).astype(
        jnp.bfloat16
    )
    latent_columns = query_latent.shape[1]
    shard_rows = gathered_by_axis(query_small, (("ep_0", "ep_1", "ep_2"), "tp"), 0)
    columns = jnp.concatenate(
        [
            jnp.dot(shard_rows, query_latent, preferred_element_type=jnp.float32),
            jnp.dot(shard_rows, query_rope, preferred_element_type=jnp.float32),
        ],
        axis=1,
    ).astype(jnp.bfloat16)
    at_home = lax.all_to_all(columns, EP_TP, split_axis=0, concat_axis=1, tiled=True)
    at_home = at_home.reshape(sequences, devices, columns.shape[1])
    head_count = value_up.shape[1]
    query_latents = at_home[:, :, :latent_columns].reshape(sequences, head_count, -1)
    query_pe = at_home[:, :, latent_columns:].reshape(sequences, head_count, -1)
    query_rotary = rotate(query_pe.astype(jnp.float32), turns[:, None, :]).astype(jnp.bfloat16)
    mixture = attend_local(
        query_latents, query_rotary, latent_cache, rope_cache, new_latent, new_rope, lengths
    )
    values = jnp.einsum("shl,lhv->shv", mixture, value_up, preferred_element_type=jnp.float32)
    values = values.astype(jnp.bfloat16).reshape(sequences, -1)
    output_cols = jnp.dot(
        lax.all_gather(values, EP_TP, axis=0, tiled=True),
        output_weight,
        preferred_element_type=jnp.float32,
    ).astype(jnp.bfloat16)
    attended = lax.all_to_all(output_cols, EP_TP, split_axis=0, concat_axis=1, tiled=True)
    after_attention = stream + attended.astype(jnp.float32)
    second = normalize(after_attention, norm_second).astype(jnp.bfloat16)
    owners = owner_table(sequences)
    assign = sequences * TOP
    group_size = devices // EXPERTS
    weights = jax.nn.softmax(route_scores.astype(jnp.float32), axis=-1)
    matches = slot_tables(route_ids.reshape(1, assign))[0].astype(jnp.float32)
    picker = jnp.einsum("aec,sa->ecs", matches, owners).astype(jnp.bfloat16)
    outbound = jnp.einsum("ecs,sd->ecd", picker, second, preferred_element_type=jnp.float32).astype(
        jnp.bfloat16
    )
    outbound = jnp.broadcast_to(outbound[:, None], (EXPERTS, group_size, CAP, model_width))
    outbound = outbound.reshape(devices, CAP, model_width)
    arrived = lax.all_to_all(outbound, EP_TP, split_axis=0, concat_axis=0, tiled=True)
    partial_value = expert_rows(
        arrived.reshape(-1, model_width), expert_gate, expert_up, expert_down
    )
    returned = lax.all_to_all(
        partial_value.reshape(arrived.shape).astype(jnp.bfloat16),
        EP_TP,
        split_axis=0,
        concat_axis=0,
        tiled=True,
    ).astype(jnp.float32)
    summed = jnp.sum(returned.reshape(EXPERTS, group_size, CAP, model_width), axis=1)
    combine_weights = matches * weights.reshape(assign)[:, None, None]
    token_weights = jnp.einsum("aec,sa->sec", combine_weights, owners)
    routed = jnp.einsum("sec,ecd->sd", token_weights, summed)
    layer_out = (after_attention + routed).astype(jnp.bfloat16)
    return (layer_out, new_latent, new_rope)


def solution(mesh):
    torus = Mesh(mesh.devices.reshape(4, 4, 4, mesh.shape["tp"]), ("ep_0", "ep_1", "ep_2", "tp"))
    placed = (
        P(EP_TP, None),
        P(EP_TP),
        P(EP_TP, None, None),
        P(EP_TP, None, None),
        P(EP_TP, None),
        P(EP_TP, None),
        P(),
        P(),
        P(),
        P(),
        P(EP_TP, None),
        P(EP_TP, None),
        P(),
        P(None, EP_TP),
        P(None, EP_TP),
        P(),
        P(None, EP_TP),
        P(None, EP_TP),
        P(None, EP_TP),
        P(EP_TP, None),
    )
    return jax.shard_map(
        local,
        mesh=torus,
        in_specs=placed,
        out_specs=(P(EP_TP, None), P(EP_TP, None), P(EP_TP, None)),
        check_vma=False,
    )
```

profile of v0, /device:TPU:1, one launch (start us, length us, event | category | flops | bytes accessed | tf_op | source)
XLA Modules:
  0.0 437.4 jit_solution(7753741035902536983)
XLA Ops:
  9.8 20.9 %all_to_all.75 = bf16[128,2,128]{2,1,0:T(2,128)(2,1)S(1)} all-to-all(bf16[128,2,128]{2,1,0:T(2,128)(2,1)S(1)} %reshape.366), channel_id=1, replica_groups=mesh['ep_0'=4,'ep_1'=4,'ep_2'=4,'tp'=2] {'ep_0','ep_1','ep_2','tp'}, dimensions={0} | all-to-all | bytes 131072 | tf_op jit(solution)/shard_map/all_to_all | solution.py:161
  36.1 6.5 %copy.77 = f32[1024,1536]{1,0:T(8,128)} copy(f32[1024,1536]{0,1:T(8,128)} %pad_maximum_fusion) | data formatting | bytes 12582912 | tf_op jit(solution)/shard_map/concatenate | solution.py:164
  45.9 10.4 %all_to_all.76 = f32[2,64,8,1536]{3,2,1,0:T(8,128)} all-to-all(f32[2,64,8,1536]{3,2,1,0:T(8,128)S(1)} %copy.78), channel_id=1, replica_groups=mesh['ep_0'=4,'ep_1'=4,'ep_2'=4,'tp'=2] {'tp'}, dimensions={0} | all-to-all | bytes 12582912 | tf_op jit(solution)/shard_map/all_to_all | solution.py:24
  56.2 5.4 %reduce_sum.91 = f32[64,8,1536]{2,1,0:T(8,128)} reduce(f32[2,64,8,1536]{3,2,1,0:T(8,128)} %all_to_all.76, f32[]{:T(128)} %constant.38.clone.1), dimensions={0}, to_apply=%region_1.0 | reduce | flops 786432 | bytes 9437188 | tf_op jit(solution)/shard_map/reduce_sum | solution.py:25
  61.6 46.3 %all_to_all.77 = f32[64,8,1536]{2,1,0:T(8,128)} all-to-all(f32[64,8,1536]{2,1,0:T(8,128)} %reduce_sum.91), channel_id=1, replica_groups=mesh['ep_0'=4,'ep_1'=4,'ep_2'=4,'tp'=2] {'ep_0','ep_1','ep_2'}, dimensions={0} | all-to-all | bytes 6291456 | tf_op jit(solution)/shard_map/all_to_all | solution.py:32
  111.4 5.7 %all-to-all-start.3 = ((bf16[64,8,1024]{2,1,0:T(8,128)(2,1)}), bf16[64,8,1024]{2,1,0:T(8,128)(2,1)S(1)}, u32[]{:S(2)}, u32[]{:S(2)}) async-start(bf16[64,8,1024]{2,1,0:T(8,128)(2,1)} %broadcast_in_dim.15), calls=%async_computation.3 | async-start | bytes 2097152 | tf_op jit(solution)/shard_map/all_to_all | solution.py:38
  117.8 17.4 %all-to-all-done.3 = bf16[64,8,1024]{2,1,0:T(8,128)(2,1)S(1)} async-done(((bf16[64,8,1024]{2,1,0:T(8,128)(2,1)}), bf16[64,8,1024]{2,1,0:T(8,128)(2,1)S(1)}, u32[]{:S(2)}, u32[]{:S(2)}) %all-to-all-start.3) | async-done | bytes 1048608 | tf_op jit(solution)/shard_map/all_to_all | solution.py:38
  136.0 6.9 %all_to_all.78 = bf16[2,64,8,1024]{3,1,2,0:T(8,128)(2,1)S(1)} all-to-all(bf16[2,64,8,1024]{3,1,2,0:T(8,128)(2,1)S(1)} %broadcast_in_dim.16), channel_id=1, replica_groups=mesh['ep_0'=4,'ep_1'=4,'ep_2'=4,'tp'=2] {'tp'}, dimensions={0} | all-to-all | bytes 4194304 | tf_op jit(solution)/shard_map/all_to_all | solution.py:38
  155.9 13.6 %all-to-all-done.5 = bf16[128,8,144]{2,1,0:T(8,128)(2,1)S(1)} async-done(((bf16[128,8,144]{2,1,0:T(8,128)(2,1)}), bf16[128,8,144]{2,1,0:T(8,128)(2,1)S(1)}, u32[]{:S(2)}, u32[]{:S(2)}) %all-to-all-start.5) | async-done | bytes 294944 | tf_op jit(solution)/shard_map/all_to_all | solution.py:189
  170.8 5.9 %fusion.83 = f32[8,32,1024]{2,1,0:T(8,128)S(1)} fusion(bf16[8,32,512]{2,1,0:T(8,128)(2,1)S(1)} %reshape.347, bf16[8,1024,512]{2,1,0:T(8,128)(2,1)} %param.22), kind=kOutput, calls=%fused_computation.115 | convolution fusion | flops 268435456 | bytes 9699328 | tf_op jit(solution)/shard_map/shl,spl->shp/dot_general | solution.py:109
  177.9 5.2 %fusion.7 = bf16[8,32,512]{2,1,0:T(8,128)(2,1)S(1)} fusion(bf16[8,1024,512]{2,1,0:T(8,128)(2,1)} %param.22, f32[8,32,1024]{2,1,0:T(8,128)S(1)} %get-tuple-element.14, f32[8,32]{1,0:T(8,128)S(1)} %get-tuple-element.8, f32[8,32]{1,0:T(8,128)S(1)} %fusion.72, f32[8,512]{1,0:T(8,128)S(1)} %get-tuple-element.3, f32[8,32]{1,0:T(8,128)S(1)} %get-tuple-element.7), kind=kOutput, calls=%fused_computation.15 | convolution fusion | flops 269615104 | bytes 9718784 | tf_op jit(solution)/shard_map/shp,spl->shl/dot_general | solution.py:124
  183.1 5.2 %fusion.11 = bf16[8,4096]{1,0:T(8,128)(2,1)} fusion(bf16[512,32,128]{2,1,0:T(8,128)(2,1)S(1)} %copy-done.2, bf16[8,32,512]{2,1,0:T(8,128)(2,1)S(1)} %fusion.7), kind=kOutput, calls=%fused_computation.18 | convolution fusion | flops 33587200 | bytes 4521984 | tf_op jit(solution)/shard_map/shl,lhv->shv/dot_general | solution.py:198
  188.9 66.1 %all-gather.2.cloned.1.call-done = bf16[1024,4096]{1,0:T(8,128)(2,1)} async-done(((bf16[8,4096]{1,0:T(8,128)(2,1)}), bf16[1024,4096]{1,0:T(8,128)(2,1)}) %all-gather.2.cloned.1.call-update) | async-done | bytes 8388624 | tf_op jit(solution)/shard_map/all_gather | solution.py:201
  254.9 5.9 %convolution_convert_fusion.3 = bf16[1024,32]{0,1:T(8,128)(2,1)S(1)} fusion(bf16[1024,4096]{1,0:T(8,128)(2,1)} %all-gather.2.cloned.1.call-done, bf16[4096,32]{0,1:T(8,128)(2,1)S(1)} %copy-done.6), kind=kOutput, calls=%fused_computation.19 | convolution fusion | flops 268468224 | bytes 8716288 | tf_op jit(solution)/shard_map/dot_general | solution.py:200
  261.9 5.4 %all-to-all-start.6 = ((bf16[128,2,128]{2,1,0:T(2,128)(2,1)}), bf16[128,2,128]{2,1,0:T(2,128)(2,1)S(1)}, u32[]{:S(2)}, u32[]{:S(2)}) async-start(bf16[128,2,128]{2,1,0:T(2,128)(2,1)} %reshape.368), calls=%async_computation.6 | async-start | bytes 131072 | tf_op jit(solution)/shard_map/all_to_all | solution.py:205
  267.3 9.5 %all-to-all-done.6 = bf16[128,2,128]{2,1,0:T(2,128)(2,1)S(1)} async-done(((bf16[128,2,128]{2,1,0:T(2,128)(2,1)}), bf16[128,2,128]{2,1,0:T(2,128)(2,1)S(1)}, u32[]{:S(2)}, u32[]{:S(2)}) %all-to-all-start.6) | async-done | bytes 65568 | tf_op jit(solution)/shard_map/all_to_all | solution.py:205
  280.2 57.3 %all_to_all.79 = bf16[128,3,4096]{2,1,0:T(4,128)(2,1)} all-to-all(bf16[128,3,4096]{2,1,0:T(4,128)(2,1)S(1)} %bitcast.84), channel_id=1, replica_groups=mesh['ep_0'=4,'ep_1'=4,'ep_2'=4,'tp'=2] {'ep_0','ep_1','ep_2','tp'}, dimensions={0} | all-to-all | bytes 6291456 | tf_op jit(solution)/shard_map/all_to_all | solution.py:219
  337.5 7.4 %reshape.350 = bf16[384,4096]{1,0:T(8,128)(2,1)} reshape(bf16[128,3,4096]{2,1,0:T(4,128)(2,1)} %all_to_all.79) | data formatting | bytes 6291456 | tf_op jit(solution)/shard_map/reshape | solution.py:221
  344.9 5.1 %fusion.85 = f32[384,448]{0,1:T(8,128)S(1)} fusion(bf16[384,4096]{1,0:T(8,128)(2,1)} %reshape.350, bf16[4096,448]{0,1:T(8,128)(2,1)} %param.37), kind=kOutput, calls=%fused_computation.117 | convolution fusion | flops 1409286144 | bytes 7503872 | tf_op jit(solution)/shard_map/dot_general | solution.py:98
  350.0 9.6 %convolution_convert_fusion = bf16[384,4096]{1,0:T(8,128)(2,1)} fusion(bf16[448,4096]{1,0:T(8,128)(2,1)} %param.39, bf16[384,4096]{1,0:T(8,128)(2,1)} %reshape.350, bf16[4096,448]{0,1:T(8,128)(2,1)} %param.38, f32[384,448]{0,1:T(8,128)S(1)} %fusion.85), kind=kOutput, calls=%fused_computation.2 | convolution fusion | flops 2821177344 | bytes 14319616 | tf_op jit(solution)/shard_map/dot_general | solution.py:101
  359.6 7.1 %convert_element_type.144 = bf16[128,3,4096]{2,1,0:T(4,128)(2,1)} reshape(bf16[384,4096]{1,0:T(8,128)(2,1)} %convolution_convert_fusion) | data formatting | bytes 6291456 | tf_op jit(solution)/shard_map/convert_element_type | solution.py:224
  366.7 5.6 %all-to-all-start.8 = ((bf16[128,3,4096]{2,1,0:T(4,128)(2,1)}), bf16[128,3,4096]{2,1,0:T(4,128)(2,1)}, u32[]{:S(2)}, u32[]{:S(2)}) async-start(bf16[128,3,4096]{2,1,0:T(4,128)(2,1)} %convert_element_type.144), calls=%async_computation.8 | async-start | bytes 8388608 | tf_op jit(solution)/shard_map/all_to_all | solution.py:223
  373.3 51.8 %all-to-all-done.8 = bf16[128,3,4096]{2,1,0:T(4,128)(2,1)} async-done(((bf16[128,3,4096]{2,1,0:T(4,128)(2,1)}), bf16[128,3,4096]{2,1,0:T(4,128)(2,1)}, u32[]{:S(2)}, u32[]{:S(2)}) %all-to-all-start.8) | async-done | bytes 3145760 | tf_op jit(solution)/shard_map/all_to_all | solution.py:223
  425.1 4.4 %convert_reduce_fusion = bf16[8,3,4096]{2,1,0:T(4,128)(2,1)S(1)} fusion(bf16[128,3,4096]{2,1,0:T(4,128)(2,1)} %all-to-all-done.8), kind=kLoop, calls=%fused_computation | loop fusion | flops 3047424 | bytes 3342336 | tf_op jit(solution)/shard_map/reduce_sum | solution.py:230
  (109 shorter events, 38.2 us)
Async XLA Ops:
  7.2 169.9 %copy-start = (bf16[8,1024,64]{1,2,0:T(8,128)(2,1)S(1)}, bf16[8,1024,64]{1,2,0:T(8,128)(2,1)}, u32[]{:S(2)}) copy-start(bf16[8,1024,64]{1,2,0:T(8,128)(2,1)} %param.23) | copy-start | bytes 3145732
  7.2 24.9 %copy-start.7 = (bf16[32,1024]{1,0:T(8,128)(2,1)S(1)}, bf16[32,1024]{1,0:T(8,128)(2,1)}, u32[]{:S(2)}) copy-start(bf16[32,1024]{1,0:T(8,128)(2,1)} %param.30) | copy-start | bytes 196612
  61.6 48.6 %copy-start.11 = (f32[1024]{0:T(1024)S(1)}, f32[1024]{0:T(1024)}, u32[]{:S(2)}) copy-start(f32[1024]{0:T(1024)} %param.28) | copy-start | bytes 12292
  107.9 9.2 %copy-start.14 = (s32[8]{0:T(128)S(1)}, s32[8]{0:T(128)}, u32[]{:S(2)}) copy-start(s32[8]{0:T(128)} %param.21) | copy-start | bytes 100
  108.0 9.2 %copy-start.4 = (bf16[4096,64]{0,1:T(8,128)(2,1)S(1)}, bf16[4096,64]{0,1:T(8,128)(2,1)}, u32[]{:S(2)}) copy-start(bf16[4096,64]{0,1:T(8,128)(2,1)} %param.32) | copy-start | bytes 1572868
  111.4 23.8 %all-to-all-start.3 = ((bf16[64,8,1024]{2,1,0:T(8,128)(2,1)}), bf16[64,8,1024]{2,1,0:T(8,128)(2,1)S(1)}, u32[]{:S(2)}, u32[]{:S(2)}) async-start(bf16[64,8,1024]{2,1,0:T(8,128)(2,1)} %broadcast_in_dim.15), calls=%async_computation.3 | async-start | bytes 2097152 | tf_op jit(solution)/shard_map/all_to_all | solution.py:38
  142.9 6.3 %copy-start.8 = (bf16[1024,16]{0,1:T(8,128)(2,1)S(1)}, bf16[1024,16]{0,1:T(8,128)(2,1)}, u32[]{:S(2)}) copy-start(bf16[1024,16]{0,1:T(8,128)(2,1)} %param.34) | copy-start | bytes 98308
  146.4 3.5 copy-start.5
  149.2 6.5 %copy-start.12 = (f32[512]{0:T(512)S(1)}, f32[512]{0:T(512)}, u32[]{:S(2)}) copy-start(f32[512]{0:T(512)} %param.29) | copy-start | bytes 6148
  152.0 17.5 %all-to-all-start.5 = ((bf16[128,8,144]{2,1,0:T(8,128)(2,1)}), bf16[128,8,144]{2,1,0:T(8,128)(2,1)S(1)}, u32[]{:S(2)}, u32[]{:S(2)}) async-start(bf16[128,8,144]{2,1,0:T(8,128)(2,1)} %copy.82), calls=%async_computation.5 | async-start | bytes 1048576 | tf_op jit(solution)/shard_map/all_to_all | solution.py:189
  155.7 99.2 %all-gather.2.cloned.1.call-start = ((), (), s32[]{:S(2)}) async-start(), calls=%async_computation.9 | async-start | bytes 8454144 | tf_op jit(solution)/shard_map/all_gather | solution.py:201
  155.8 20.9 %copy-start.10 = (bf16[8,512]{1,0:T(8,128)(2,1)}, bf16[8,512]{1,0:T(8,128)(2,1)S(1)}, u32[]{:S(2)}) copy-start(bf16[8,512]{1,0:T(8,128)(2,1)S(1)} %get-tuple-element.4) | copy-start | bytes 24580
  177.9 5.2 %copy-start.2 = (bf16[512,32,128]{2,1,0:T(8,128)(2,1)S(1)}, bf16[512,32,128]{2,1,0:T(8,128)(2,1)}, u32[]{:S(2)}) copy-start(bf16[512,32,128]{2,1,0:T(8,128)(2,1)} %param.35) | copy-start | bytes 12582916
  183.1 5.3 %copy-start.13 = (s32[8,2]{0,1:T(2,128)S(1)}, s32[8,2]{0,1:T(2,128)}, u32[]{:S(2)}) copy-start(s32[8,2]{0,1:T(2,128)} %param.24) | copy-start | bytes 196
  183.1 71.8 %copy-start.6 = (bf16[4096,32]{0,1:T(8,128)(2,1)S(1)}, bf16[4096,32]{0,1:T(8,128)(2,1)}, u32[]{:S(2)}) copy-start(bf16[4096,32]{0,1:T(8,128)(2,1)} %param.36) | copy-start | bytes 786436
  188.9 88.5 %copy-start.3 = (bf16[8,4096]{1,0:T(8,128)(2,1)S(1)}, bf16[8,4096]{1,0:T(8,128)(2,1)}, u32[]{:S(2)}) copy-start(bf16[8,4096]{1,0:T(8,128)(2,1)} %param.20) | copy-start | bytes 196612
  260.9 16.7 %copy-start.9 = (f32[4096]{0:T(1024)S(1)}, f32[4096]{0:T(1024)}, u32[]{:S(2)}) copy-start(f32[4096]{0:T(1024)} %param.27) | copy-start | bytes 49156
  261.9 14.9 %all-to-all-start.6 = ((bf16[128,2,128]{2,1,0:T(2,128)(2,1)}), bf16[128,2,128]{2,1,0:T(2,128)(2,1)S(1)}, u32[]{:S(2)}, u32[]{:S(2)}) async-start(bf16[128,2,128]{2,1,0:T(2,128)(2,1)} %reshape.368), calls=%async_computation.6 | async-start | bytes 131072 | tf_op jit(solution)/shard_map/all_to_all | solution.py:205
  366.7 5.7 %copy-start.15 = (bf16[8,2]{0,1:T(2,128)(2,1)S(1)}, bf16[8,2]{0,1:T(2,128)(2,1)}, u32[]{:S(2)}) copy-start(bf16[8,2]{0,1:T(2,128)(2,1)} %param.25) | copy-start | bytes 100
  366.7 58.4 %all-to-all-start.8 = ((bf16[128,3,4096]{2,1,0:T(4,128)(2,1)}), bf16[128,3,4096]{2,1,0:T(4,128)(2,1)}, u32[]{:S(2)}, u32[]{:S(2)}) async-start(bf16[128,3,4096]{2,1,0:T(4,128)(2,1)} %convert_element_type.144), calls=%async_computation.8 | async-start | bytes 8388608 | tf_op jit(solution)/shard_map/all_to_all | solution.py:223
  372.4 58.2 %copy-start.1 = (bf16[8,1024,64]{1,2,0:T(8,128)(2,1)S(1)}, bf16[8,1024,64]{1,2,0:T(8,128)(2,1)}, u32[]{:S(2)}) copy-start(bf16[8,1024,64]{1,2,0:T(8,128)(2,1)} %param.23) | copy-start | bytes 3145732
Sparse Core Ops, SparseCore 0:
  188.5 66.3 all-gather.1
where the time goes:
time: 439 us; the launch traced here: 437 us
  waiting for transfers between devices  158 us (36%)
  blocking collectives  142 us (32%)
  matrix products  42.9 us (10%)
  local copies, waits for them, and re-layouts  39.7 us (9%)
  starting transfers between devices  20.5 us (5%)
  other arithmetic  19.6 us (4%)
  between operations  14.5 us (3%)
    all_gather x1, waiting for transfers between devices, local(): lax.all_gather(values, EP_TP, axis=0, tiled=True)  66.1 us
    all_to_all x1, blocking collectives, local(): lax.all_to_all(outbound, EP_TP, split_axis=0, concat_axis=0, tiled=True)  57.3 us
    all_to_all x1, waiting for transfers between devices, local(): lax.all_to_all(partial_value.reshape(arrived.shape).astype(jnp.bfloat16),...  51.8 us
    all_to_all x1, blocking collectives, sum_by_axis(): lax.all_to_all(nearer, far, split_axis=0, concat_axis=0, tiled=True)  46.3 us
    all_to_all x1, blocking collectives, local(): lax.all_to_all(normed, EP_TP, split_axis=1, concat_axis=0, tiled=True)  20.9 us
    all_to_all x1, waiting for transfers between devices, sent_to_all(): lax.all_to_all(jnp.broadcast_to(shard[None], (peers, *shard.shape)), axis...  17.4 us
    all_to_all x1, waiting for transfers between devices, local(): lax.all_to_all(columns, EP_TP, split_axis=0, concat_axis=1, tiled=True)  13.6 us
    all_to_all x1, blocking collectives, sent_and_summed(): lax.all_to_all(parts, axis, split_axis=0, concat_axis=0, tiled=True)  10.4 us
  transfers between devices with their start and end apart: 5, of which 5 were waited for; matrix products, arithmetic and copies ran while one was open for 0% of the time, Pallas kernels for 0%

commit v1 on v0

--- a/solution.py
+++ b/solution.py
@@ -198,7 +198,9 @@
     values = jnp.einsum("shl,lhv->shv", mixture, value_up, preferred_element_type=jnp.float32)
     values = values.astype(jnp.bfloat16).reshape(sequences, -1)
     output_cols = jnp.dot(
-        lax.all_gather(values, EP_TP, axis=0, tiled=True),
+        jnp.concatenate(
+            lax.all_to_all(jnp.stack([values] * lax.axis_size(EP_TP)), EP_TP, 0, 0), axis=0
+        ),
         output_weight,
         preferred_element_type=jnp.float32,
     ).astype(jnp.bfloat16)

time: 439 us -> 492 us (1.12); the launches traced: 437 us -> 484 us
  waiting for transfers between devices: 158 us -> 191 us
  between operations: 14.5 us -> 1.5 us
  starting transfers between devices: 20.5 us -> 32.6 us
  blocking collectives: 142 us -> 153 us
    all_to_all x0 -> x1, waiting for transfers between devices: none -> 98.7 us  [local(): lax.all_to_all(jnp.stack([values] * lax.axis_size(EP_TP)), EP_TP, 0, 0)]
    all_gather x1 -> x0, waiting for transfers between devices: 66.1 us -> none  [local(): lax.all_gather(values, EP_TP, axis=0, tiled=True)]
    all_to_all x1, blocking collectives: 6.9 us -> 18.3 us  [sent_to_all(): lax.all_to_all(jnp.broadcast_to(shard[None], (peers, *shard.shape)), axis...]
    all_to_all x1, starting transfers between devices: 5.36 us -> 11.8 us  [local(): lax.all_to_all(output_cols, EP_TP, split_axis=0, concat_axis=1, tiled=True)]
    all_to_all x0 -> x1, starting transfers between devices: none -> 5.75 us  [local(): lax.all_to_all(jnp.stack([values] * lax.axis_size(EP_TP)), EP_TP, 0, 0)]
where the time goes in v1:
time: 492 us; the launch traced here: 484 us
  waiting for transfers between devices  191 us (39%)
  blocking collectives  153 us (31%)
  local copies, waits for them, and re-layouts  43.9 us (9%)
  matrix products  42.3 us (9%)
  starting transfers between devices  32.6 us (7%)
  other arithmetic  19.6 us (4%)
    all_to_all x1, waiting for transfers between devices, local(): lax.all_to_all(jnp.stack([values] * lax.axis_size(EP_TP)), EP_TP, 0, 0)  98.7 us
    all_to_all x1, blocking collectives, local(): lax.all_to_all(outbound, EP_TP, split_axis=0, concat_axis=0, tiled=True)  57.3 us
    all_to_all x1, waiting for transfers between devices, local(): lax.all_to_all(partial_value.reshape(arrived.shape).astype(jnp.bfloat16),...  51.8 us
    all_to_all x1, blocking collectives, sum_by_axis(): lax.all_to_all(nearer, far, split_axis=0, concat_axis=0, tiled=True)  46.3 us
    all_to_all x1, blocking collectives, local(): lax.all_to_all(normed, EP_TP, split_axis=1, concat_axis=0, tiled=True)  20.9 us
    all_to_all x1, blocking collectives, sent_to_all(): lax.all_to_all(jnp.broadcast_to(shard[None], (peers, *shard.shape)), axis...  18.3 us
    all_to_all x1, waiting for transfers between devices, sent_to_all(): lax.all_to_all(jnp.broadcast_to(shard[None], (peers, *shard.shape)), axis...  17.4 us
    all_to_all x1, waiting for transfers between devices, local(): lax.all_to_all(columns, EP_TP, split_axis=0, concat_axis=1, tiled=True)  13.6 us
  transfers between devices with their start and end apart: 5, of which 5 were waited for; matrix products, arithmetic and copies ran while one was open for 0% of the time, Pallas kernels for 0%

profile of v1, /device:TPU:1, one launch (start us, length us, event | category | flops | bytes accessed | tf_op | source)
XLA Modules:
  0.0 484.2 jit_solution(4596341259302113633)
XLA Ops:
  3.2 20.9 %all_to_all.80 = bf16[128,2,128]{2,1,0:T(2,128)(2,1)S(1)} all-to-all(bf16[128,2,128]{2,1,0:T(2,128)(2,1)S(1)} %reshape.368), channel_id=1, replica_groups=mesh['ep_0'=4,'ep_1'=4,'ep_2'=4,'tp'=2] {'ep_0','ep_1','ep_2','tp'}, dimensions={0} | all-to-all | bytes 131072 | tf_op jit(solution)/shard_map/all_to_all | solution.py:161
  29.6 6.5 %copy.77 = f32[1024,1536]{1,0:T(8,128)} copy(f32[1024,1536]{0,1:T(8,128)} %pad_maximum_fusion) | data formatting | bytes 12582912 | tf_op jit(solution)/shard_map/concatenate | solution.py:164
  39.4 10.4 %all_to_all.81 = f32[2,64,8,1536]{3,2,1,0:T(8,128)} all-to-all(f32[2,64,8,1536]{3,2,1,0:T(8,128)S(1)} %copy.78), channel_id=1, replica_groups=mesh['ep_0'=4,'ep_1'=4,'ep_2'=4,'tp'=2] {'tp'}, dimensions={0} | all-to-all | bytes 12582912 | tf_op jit(solution)/shard_map/all_to_all | solution.py:24
  49.8 5.4 %reduce_sum.91 = f32[64,8,1536]{2,1,0:T(8,128)} reduce(f32[2,64,8,1536]{3,2,1,0:T(8,128)} %all_to_all.81, f32[]{:T(128)} %constant.38.clone.1), dimensions={0}, to_apply=%region_1.0 | reduce | flops 786432 | bytes 9437188 | tf_op jit(solution)/shard_map/reduce_sum | solution.py:25
  55.2 46.3 %all_to_all.82 = f32[64,8,1536]{2,1,0:T(8,128)} all-to-all(f32[64,8,1536]{2,1,0:T(8,128)} %reduce_sum.91), channel_id=1, replica_groups=mesh['ep_0'=4,'ep_1'=4,'ep_2'=4,'tp'=2] {'ep_0','ep_1','ep_2'}, dimensions={0} | all-to-all | bytes 6291456 | tf_op jit(solution)/shard_map/all_to_all | solution.py:32
  104.9 5.7 %all-to-all-start.3 = ((bf16[64,8,1024]{2,1,0:T(8,128)(2,1)}), bf16[64,8,1024]{2,1,0:T(8,128)(2,1)S(1)}, u32[]{:S(2)}, u32[]{:S(2)}) async-start(bf16[64,8,1024]{2,1,0:T(8,128)(2,1)} %broadcast_in_dim.15), calls=%async_computation.3 | async-start | bytes 2097152 | tf_op jit(solution)/shard_map/all_to_all | solution.py:38
  111.3 17.4 %all-to-all-done.3 = bf16[64,8,1024]{2,1,0:T(8,128)(2,1)S(1)} async-done(((bf16[64,8,1024]{2,1,0:T(8,128)(2,1)}), bf16[64,8,1024]{2,1,0:T(8,128)(2,1)S(1)}, u32[]{:S(2)}, u32[]{:S(2)}) %all-to-all-start.3) | async-done | bytes 1048608 | tf_op jit(solution)/shard_map/all_to_all | solution.py:38
  129.6 18.3 %all_to_all.83 = bf16[2,64,8,1024]{3,1,2,0:T(8,128)(2,1)S(1)} all-to-all(bf16[2,64,8,1024]{3,1,2,0:T(8,128)(2,1)S(1)} %broadcast_in_dim.16), channel_id=1, replica_groups=mesh['ep_0'=4,'ep_1'=4,'ep_2'=4,'tp'=2] {'tp'}, dimensions={0} | all-to-all | bytes 4194304 | tf_op jit(solution)/shard_map/all_to_all | solution.py:38
  160.6 13.6 %all-to-all-done.5 = bf16[128,8,144]{2,1,0:T(8,128)(2,1)S(1)} async-done(((bf16[128,8,144]{2,1,0:T(8,128)(2,1)}), bf16[128,8,144]{2,1,0:T(8,128)(2,1)S(1)}, u32[]{:S(2)}, u32[]{:S(2)}) %all-to-all-start.5) | async-done | bytes 294944 | tf_op jit(solution)/shard_map/all_to_all | solution.py:189
  175.5 5.9 %fusion.88 = f32[8,32,1024]{2,1,0:T(8,128)S(1)} fusion(bf16[8,32,512]{2,1,0:T(8,128)(2,1)S(1)} %reshape.349, bf16[8,1024,512]{2,1,0:T(8,128)(2,1)} %param.22), kind=kOutput, calls=%fused_computation.117 | convolution fusion | flops 268435456 | bytes 9699328 | tf_op jit(solution)/shard_map/shl,spl->shp/dot_general | solution.py:109
  182.7 5.2 %fusion.9 = bf16[8,32,512]{2,1,0:T(8,128)(2,1)S(1)} fusion(bf16[8,1024,512]{2,1,0:T(8,128)(2,1)} %param.22, f32[8,32,1024]{2,1,0:T(8,128)S(1)} %get-tuple-element.14, f32[8,32]{1,0:T(8,128)S(1)} %get-tuple-element.8, f32[8,32]{1,0:T(8,128)S(1)} %fusion.77, f32[8,512]{1,0:T(8,128)S(1)} %get-tuple-element.3, f32[8,32]{1,0:T(8,128)S(1)} %get-tuple-element.7), kind=kOutput, calls=%fused_computation.17 | convolution fusion | flops 269615104 | bytes 9718784 | tf_op jit(solution)/shard_map/shp,spl->shl/dot_general | solution.py:124
  187.9 4.6 fusion.13
  196.8 5.7 %all-to-all-start.6 = ((bf16[128,8,4096]{2,1,0:T(8,128)(2,1)}), bf16[128,8,4096]{2,1,0:T(8,128)(2,1)}, u32[]{:S(2)}, u32[]{:S(2)}) async-start(bf16[128,8,4096]{2,1,0:T(8,128)(2,1)} %stack.3), calls=%async_computation.6 | async-start | bytes 16777216 | tf_op jit(solution)/shard_map/all_to_all | solution.py:202
  203.0 98.7 %all-to-all-done.6 = bf16[128,8,4096]{2,1,0:T(8,128)(2,1)} async-done(((bf16[128,8,4096]{2,1,0:T(8,128)(2,1)}), bf16[128,8,4096]{2,1,0:T(8,128)(2,1)}, u32[]{:S(2)}, u32[]{:S(2)}) %all-to-all-start.6) | async-done | bytes 8388640 | tf_op jit(solution)/shard_map/all_to_all | solution.py:202
  301.8 6.0 %fusion.16 = bf16[1024,32]{0,1:T(8,128)(2,1)S(1)} fusion(bf16[4096,32]{0,1:T(8,128)(2,1)S(1)} %copy-done.6, bf16[128,8,4096]{2,1,0:T(8,128)(2,1)} %all-to-all-done.6), kind=kOutput, calls=%fused_computation.21 | convolution fusion | flops 268468224 | bytes 8716288 | tf_op jit(solution)/shard_map/dot_general | solution.py:200
  308.7 11.8 %all-to-all-start.7 = ((bf16[128,2,128]{2,1,0:T(2,128)(2,1)}), bf16[128,2,128]{2,1,0:T(2,128)(2,1)S(1)}, u32[]{:S(2)}, u32[]{:S(2)}) async-start(bf16[128,2,128]{2,1,0:T(2,128)(2,1)} %reshape.370), calls=%async_computation.7 | async-start | bytes 131072 | tf_op jit(solution)/shard_map/all_to_all | solution.py:207
  320.5 9.5 %all-to-all-done.7 = bf16[128,2,128]{2,1,0:T(2,128)(2,1)S(1)} async-done(((bf16[128,2,128]{2,1,0:T(2,128)(2,1)}), bf16[128,2,128]{2,1,0:T(2,128)(2,1)S(1)}, u32[]{:S(2)}, u32[]{:S(2)}) %all-to-all-start.7) | async-done | bytes 65568 | tf_op jit(solution)/shard_map/all_to_all | solution.py:207
  333.4 57.3 %all_to_all.84 = bf16[128,3,4096]{2,1,0:T(4,128)(2,1)} all-to-all(bf16[128,3,4096]{2,1,0:T(4,128)(2,1)S(1)} %bitcast.88), channel_id=1, replica_groups=mesh['ep_0'=4,'ep_1'=4,'ep_2'=4,'tp'=2] {'ep_0','ep_1','ep_2','tp'}, dimensions={0} | all-to-all | bytes 6291456 | tf_op jit(solution)/shard_map/all_to_all | solution.py:221
  390.8 7.4 %reshape.352 = bf16[384,4096]{1,0:T(8,128)(2,1)} reshape(bf16[128,3,4096]{2,1,0:T(4,128)(2,1)} %all_to_all.84) | data formatting | bytes 6291456 | tf_op jit(solution)/shard_map/reshape | solution.py:223
  398.2 5.1 %fusion.90 = f32[384,448]{0,1:T(8,128)S(1)} fusion(bf16[384,4096]{1,0:T(8,128)(2,1)} %reshape.352, bf16[4096,448]{0,1:T(8,128)(2,1)} %param.37), kind=kOutput, calls=%fused_computation.119 | convolution fusion | flops 1409286144 | bytes 7503872 | tf_op jit(solution)/shard_map/dot_general | solution.py:98
  403.3 9.6 %convolution_convert_fusion = bf16[384,4096]{1,0:T(8,128)(2,1)} fusion(bf16[448,4096]{1,0:T(8,128)(2,1)} %param.39, bf16[384,4096]{1,0:T(8,128)(2,1)} %reshape.352, bf16[4096,448]{0,1:T(8,128)(2,1)} %param.38, f32[384,448]{0,1:T(8,128)S(1)} %fusion.90), kind=kOutput, calls=%fused_computation.4 | convolution fusion | flops 2821177344 | bytes 14319616 | tf_op jit(solution)/shard_map/dot_general | solution.py:101
  412.9 7.1 %convert_element_type.144 = bf16[128,3,4096]{2,1,0:T(4,128)(2,1)} reshape(bf16[384,4096]{1,0:T(8,128)(2,1)} %convolution_convert_fusion) | data formatting | bytes 6291456 | tf_op jit(solution)/shard_map/convert_element_type | solution.py:226
  420.0 5.6 %all-to-all-start.9 = ((bf16[128,3,4096]{2,1,0:T(4,128)(2,1)}), bf16[128,3,4096]{2,1,0:T(4,128)(2,1)}, u32[]{:S(2)}, u32[]{:S(2)}) async-start(bf16[128,3,4096]{2,1,0:T(4,128)(2,1)} %convert_element_type.144), calls=%async_computation.9 | async-start | bytes 8388608 | tf_op jit(solution)/shard_map/all_to_all | solution.py:225
  426.6 51.8 %all-to-all-done.9 = bf16[128,3,4096]{2,1,0:T(4,128)(2,1)} async-done(((bf16[128,3,4096]{2,1,0:T(4,128)(2,1)}), bf16[128,3,4096]{2,1,0:T(4,128)(2,1)}, u32[]{:S(2)}, u32[]{:S(2)}) %all-to-all-start.9) | async-done | bytes 3145760 | tf_op jit(solution)/shard_map/all_to_all | solution.py:225
  (109 shorter events, 46.8 us)
Async XLA Ops:
  0.6 181.3 %copy-start = (bf16[8,1024,64]{1,2,0:T(8,128)(2,1)S(1)}, bf16[8,1024,64]{1,2,0:T(8,128)(2,1)}, u32[]{:S(2)}) copy-start(bf16[8,1024,64]{1,2,0:T(8,128)(2,1)} %param.23) | copy-start | bytes 3145732
  0.6 25.3 %copy-start.7 = (bf16[32,512]{1,0:T(8,128)(2,1)S(1)}, bf16[32,512]{1,0:T(8,128)(2,1)}, u32[]{:S(2)}) copy-start(bf16[32,512]{1,0:T(8,128)(2,1)} %param.31) | copy-start | bytes 98308
  55.2 48.6 %copy-start.11 = (f32[1024]{0:T(1024)S(1)}, f32[1024]{0:T(1024)}, u32[]{:S(2)}) copy-start(f32[1024]{0:T(1024)} %param.28) | copy-start | bytes 12292
  101.5 9.2 %copy-start.14 = (s32[8]{0:T(128)S(1)}, s32[8]{0:T(128)}, u32[]{:S(2)}) copy-start(s32[8]{0:T(128)} %param.21) | copy-start | bytes 100
  101.5 9.2 %copy-start.4 = (bf16[4096,64]{0,1:T(8,128)(2,1)S(1)}, bf16[4096,64]{0,1:T(8,128)(2,1)}, u32[]{:S(2)}) copy-start(bf16[4096,64]{0,1:T(8,128)(2,1)} %param.32) | copy-start | bytes 1572868
  104.9 23.8 %all-to-all-start.3 = ((bf16[64,8,1024]{2,1,0:T(8,128)(2,1)}), bf16[64,8,1024]{2,1,0:T(8,128)(2,1)S(1)}, u32[]{:S(2)}, u32[]{:S(2)}) async-start(bf16[64,8,1024]{2,1,0:T(8,128)(2,1)} %broadcast_in_dim.15), calls=%async_computation.3 | async-start | bytes 2097152 | tf_op jit(solution)/shard_map/all_to_all | solution.py:38
  147.8 6.3 %copy-start.5 = (bf16[1024,128]{1,0:T(8,128)(2,1)S(1)}, bf16[1024,128]{1,0:T(8,128)(2,1)}, u32[]{:S(2)}) copy-start(bf16[1024,128]{1,0:T(8,128)(2,1)} %param.33) | copy-start | bytes 786436
  151.3 3.6 copy-start.8
  154.1 6.4 %copy-start.12 = (f32[512]{0:T(512)S(1)}, f32[512]{0:T(512)}, u32[]{:S(2)}) copy-start(f32[512]{0:T(512)} %param.29) | copy-start | bytes 6148
  156.8 17.4 %all-to-all-start.5 = ((bf16[128,8,144]{2,1,0:T(8,128)(2,1)}), bf16[128,8,144]{2,1,0:T(8,128)(2,1)S(1)}, u32[]{:S(2)}, u32[]{:S(2)}) async-start(bf16[128,8,144]{2,1,0:T(8,128)(2,1)} %copy.82), calls=%async_computation.5 | async-start | bytes 1048576 | tf_op jit(solution)/shard_map/all_to_all | solution.py:189
  160.6 20.7 %copy-start.10 = (bf16[8,512]{1,0:T(8,128)(2,1)}, bf16[8,512]{1,0:T(8,128)(2,1)S(1)}, u32[]{:S(2)}) copy-start(bf16[8,512]{1,0:T(8,128)(2,1)S(1)} %get-tuple-element.4) | copy-start | bytes 24580
  182.7 5.2 %copy-start.2 = (bf16[512,32,128]{2,1,0:T(8,128)(2,1)S(1)}, bf16[512,32,128]{2,1,0:T(8,128)(2,1)}, u32[]{:S(2)}) copy-start(bf16[512,32,128]{2,1,0:T(8,128)(2,1)} %param.35) | copy-start | bytes 12582916
  196.8 5.8 %copy-start.13 = (s32[8,2]{0,1:T(2,128)S(1)}, s32[8,2]{0,1:T(2,128)}, u32[]{:S(2)}) copy-start(s32[8,2]{0,1:T(2,128)} %param.24) | copy-start | bytes 196
  196.8 105.0 %copy-start.6 = (bf16[4096,32]{0,1:T(8,128)(2,1)S(1)}, bf16[4096,32]{0,1:T(8,128)(2,1)}, u32[]{:S(2)}) copy-start(bf16[4096,32]{0,1:T(8,128)(2,1)} %param.36) | copy-start | bytes 786436
  196.8 105.0 %all-to-all-start.6 = ((bf16[128,8,4096]{2,1,0:T(8,128)(2,1)}), bf16[128,8,4096]{2,1,0:T(8,128)(2,1)}, u32[]{:S(2)}, u32[]{:S(2)}) async-start(bf16[128,8,4096]{2,1,0:T(8,128)(2,1)} %stack.3), calls=%async_computation.6 | async-start | bytes 16777216 | tf_op jit(solution)/shard_map/all_to_all | solution.py:202
  203.0 127.6 %copy-start.3 = (bf16[8,4096]{1,0:T(8,128)(2,1)S(1)}, bf16[8,4096]{1,0:T(8,128)(2,1)}, u32[]{:S(2)}) copy-start(bf16[8,4096]{1,0:T(8,128)(2,1)} %param.20) | copy-start | bytes 196612
  307.7 23.1 %copy-start.9 = (f32[4096]{0:T(1024)S(1)}, f32[4096]{0:T(1024)}, u32[]{:S(2)}) copy-start(f32[4096]{0:T(1024)} %param.27) | copy-start | bytes 49156
  308.7 21.4 %all-to-all-start.7 = ((bf16[128,2,128]{2,1,0:T(2,128)(2,1)}), bf16[128,2,128]{2,1,0:T(2,128)(2,1)S(1)}, u32[]{:S(2)}, u32[]{:S(2)}) async-start(bf16[128,2,128]{2,1,0:T(2,128)(2,1)} %reshape.370), calls=%async_computation.7 | async-start | bytes 131072 | tf_op jit(solution)/shard_map/all_to_all | solution.py:207
  420.0 5.7 %copy-start.15 = (bf16[8,2]{0,1:T(2,128)(2,1)S(1)}, bf16[8,2]{0,1:T(2,128)(2,1)}, u32[]{:S(2)}) copy-start(bf16[8,2]{0,1:T(2,128)(2,1)} %param.25) | copy-start | bytes 100
  420.0 58.4 %all-to-all-start.9 = ((bf16[128,3,4096]{2,1,0:T(4,128)(2,1)}), bf16[128,3,4096]{2,1,0:T(4,128)(2,1)}, u32[]{:S(2)}, u32[]{:S(2)}) async-start(bf16[128,3,4096]{2,1,0:T(4,128)(2,1)} %convert_element_type.144), calls=%async_computation.9 | async-start | bytes 8388608 | tf_op jit(solution)/shard_map/all_to_all | solution.py:225
  425.7 58.2 %copy-start.1 = (bf16[8,1024,64]{1,2,0:T(8,128)(2,1)S(1)}, bf16[8,1024,64]{1,2,0:T(8,128)(2,1)}, u32[]{:S(2)}) copy-start(bf16[8,1024,64]{1,2,0:T(8,128)(2,1)} %param.23) | copy-start | bytes 3145732
